TPU v7x, 32 devices: a whole 2x2x4 slice. The times are simulated.
32 devices in a mesh: grp: 2 (over y), ep: 4 (over z), tp: 4 (over x, core).
Axes of the slice: x: 2, y: 2, z: 4, core: 2. Of those that a mesh axis runs over, the one named last changes fastest.
Arguments:
- tokens: bfloat16 [2048, 2048], P(('grp', 'ep')), parts along dimension 0, may hold values from -6 to 6
- norm_gain: float32 [2048], replicated, may hold values from 0.1 to 1.9
- routing: int32 [2048, 2], P(('grp', 'ep')), parts along dimension 0, may hold values from 0 to 3, all different within a row; in each aligned block of 256 rows (0 to 255, 256 to 511, ...) at most 192 rows name the same one
- gate_weights: float32 [2048, 2], P(('grp', 'ep')), parts along dimension 0, may hold values from 0.2 to 2
- expert_gate: bfloat16 [4, 2048, 1024], P('ep', None, 'tp'), may hold values from -0.125 to 0.125
- expert_up: bfloat16 [4, 2048, 1024], P('ep', None, 'tp'), may hold values from -0.125 to 0.125
- expert_down: bfloat16 [4, 1024, 2048], P('ep', 'tp'), may hold values from -0.1875 to 0.1875
- shared_gate: bfloat16 [2048, 512], P(None, 'tp'), may hold values from -0.125 to 0.125
- shared_up: bfloat16 [2048, 512], P(None, 'tp'), may hold values from -0.125 to 0.125
- shared_down: bfloat16 [512, 2048], P('tp'), may hold values from -0.25 to 0.25
Outputs:
- mixed: bfloat16 [2048, 2048], P(('grp', 'ep'), 'tp'), parts along dimension 0
There are 2 independent parts, one for each index of `grp`. A program takes and returns all parts, laid end to end along the dimension named above; an argument that names none is the same for every part. Nothing has to cross between parts.
Inputs may be any that keep to these rules, and one draw needn't show every extreme that they name: `routing`: each row names 2 different experts. Within each aligned block of 256 rows no expert is named by more than 192 rows, and in every draw some block has an expert named by exactly 192 rows.
All inputs are finite; a program needn't handle non-finite values.
Results may differ from a plain program's by a relative error of at most 0.012.
Values may be sent and summed in bfloat16 or wider, within the bound.
A program may use at most 64 MiB of HBM per device.

v0:
```python
import jax
import jax.numpy as jnp
from jax import lax
from jax.sharding import PartitionSpec as P


def norm_rows(tokens, norm_gain):
    values = tokens.astype(jnp.float32)
    scale = lax.rsqrt(jnp.mean(values * values, axis=-1, keepdims=True) + 1e-06)
    return (values * scale * norm_gain).astype(jnp.bfloat16)


def body(
    tokens,
    norm_gain,
    routing,
    gate_weights,
    expert_gate,
    expert_up,
    expert_down,
    shared_gate,
    shared_up,
    shared_down,
):
    ep_count = lax.axis_size("ep")
    tp_count = lax.axis_size("tp")
    tok_rows, width = tokens.shape
    top = routing.shape[1]
    local_experts = expert_gate.shape[0]
    experts = ep_count * local_experts
    capacity = max(2, 3 * tok_rows * top // (2 * experts))
    quarter = width // tp_count
    arrived_rows = ep_count * capacity
    normed = norm_rows(tokens, norm_gain)
    flat_experts = routing.reshape(-1)
    assign = flat_experts.shape[0]
    onehot = (flat_experts[:, None] == jnp.arange(experts, dtype=jnp.int32)[None, :]).astype(
        jnp.float32
    )
    lower = (jnp.arange(assign)[:, None] >= jnp.arange(assign)[None, :]).astype(jnp.float32)
    running = jnp.dot(lower, onehot, precision=lax.Precision.HIGHEST)
    slot = (jnp.sum(running * onehot, axis=1) - 1.0).astype(jnp.int32)
    dest = flat_experts * capacity + slot
    owner = jnp.arange(assign, dtype=jnp.int32) // top
    slot_token = jnp.full((experts * capacity,), tok_rows, jnp.int32).at[dest].set(owner)
    padded = jnp.concatenate([normed, jnp.zeros((1, width), jnp.bfloat16)], axis=0)
    outgoing = padded[slot_token].reshape(experts, capacity, width)
    position = lax.axis_index("tp")
    own_columns = lax.dynamic_slice_in_dim(outgoing, position * quarter, quarter, 2)
    arrived = lax.all_to_all(own_columns, "ep", split_axis=0, concat_axis=0, tiled=True)
    piece = lax.all_gather(arrived, "tp", axis=2, tiled=True)
    count = piece.shape[2]
    piece = piece.reshape(ep_count, local_experts, capacity, count)
    local = 0
    rows = piece[:, local].reshape(arrived_rows, count)
    gate_rows = expert_gate[local]
    up_rows = expert_up[local]
    gate_list = [jnp.dot(rows, gate_rows, preferred_element_type=jnp.float32)]
    up_list = [jnp.dot(rows, up_rows, preferred_element_type=jnp.float32)]
    gate_all = jnp.stack(gate_list)
    up_all = jnp.stack(up_list)
    local = 0
    hidden = (jax.nn.silu(gate_all[local]) * up_all[local]).astype(jnp.bfloat16)
    term = jnp.dot(hidden, expert_down[local], preferred_element_type=jnp.float32)
    routed_list = [term.reshape(ep_count, capacity, width)]
    routed_terms = jnp.stack(routed_list, axis=1).reshape(experts * capacity, width)
    shared_gate_rows = jnp.dot(normed, shared_gate, preferred_element_type=jnp.float32)
    shared_up_rows = jnp.dot(normed, shared_up, preferred_element_type=jnp.float32)
    shared_hidden = (jax.nn.silu(shared_gate_rows) * shared_up_rows).astype(jnp.bfloat16)
    shared_term = jnp.dot(shared_hidden, shared_down, preferred_element_type=jnp.float32)
    routed_sum, shared_sum = (
        lax.psum_scatter(
            routed_terms.astype(jnp.bfloat16), "tp", scatter_dimension=1, tiled=True
        ).astype(jnp.float32),
        lax.psum_scatter(
            shared_term.astype(jnp.bfloat16), "tp", scatter_dimension=1, tiled=True
        ).astype(jnp.float32),
    )
    expert_out = routed_sum.astype(jnp.bfloat16).reshape(experts, capacity, quarter)
    returned = lax.all_to_all(expert_out, "ep", split_axis=0, concat_axis=0, tiled=True)
    picked = returned.reshape(experts * capacity, quarter)[dest]
    picked = picked.astype(jnp.float32).reshape(tok_rows, top, quarter)
    routed = jnp.sum(picked * gate_weights[:, :, None], axis=1)
    return (routed + shared_sum).astype(jnp.bfloat16)


def solution(mesh):
    in_specs = (
        P(("grp", "ep"), None),
        P(),
        P(("grp", "ep"), None),
        P(("grp", "ep"), None),
        P("ep", None, "tp"),
        P("ep", None, "tp"),
        P("ep", "tp", None),
        P(None, "tp"),
        P(None, "tp"),
        P("tp", None),
    )
    out_specs = P(("grp", "ep"), "tp")
    return jax.shard_map(body, mesh=mesh, in_specs=in_specs, out_specs=out_specs, check_vma=False)
```

profile of v0, /device:TPU:0, one launch (start us, length us, event | category | flops | bytes accessed | tf_op | source)
XLA Modules:
  0.0 160.1 jit_solution(5352269247419318608)
XLA Ops:
  6.5 0.0 copy-start
  6.5 0.0 all-gather.2.cloned.1.call-start
  6.5 0.8 broadcast_multiply_fusion
  7.3 0.8 copy.13
  8.1 1.5 fusion
  9.7 0.1 copy.12
  9.8 0.1 mul.70
  9.9 0.1 eq.15
  10.1 0.3 fusion.5
  10.4 2.4 %scatter_custom_fusion = s32[768]{0:T(1024)S(1)} fusion(s32[512]{0:T(512)S(1)} %bitcast.27, s32[512]{0:T(512)S(1)} %add_select_fusion, s32[]{:T(128)} %constant.23.clone.1), kind=kCustom, calls=%fused_computation.48 | custom fusion | bytes 3076 | tf_op jit(solution)/shard_map/scatter | solution.py:45
  12.9 1.5 fusion.2
  14.4 0.1 concatenate.3
  14.5 4.3 %gather_fusion = bf16[768,2048]{1,0:T(8,128)(2,1)} fusion(bf16[257,2048]{1,0:T(8,128)(2,1)S(1)} %concatenate.3, s32[1024]{0:T(1024)S(1)} %pad_clamp_fusion.1), kind=kCustom, calls=%fused_computation | custom fusion | bytes 6294528 | tf_op jit(solution)/shard_map/gather | solution.py:47
  18.8 0.0 copy-start.4
  18.8 1.3 constant_dynamic-slice_fusion
  20.1 26.4 %all_to_all.10 = bf16[4,192,512]{2,1,0:T(8,128)(2,1)} all-to-all(bf16[4,192,512]{2,1,0:T(8,128)(2,1)S(1)} %constant_dynamic-slice_fusion), channel_id=1, replica_groups=mesh['grp'=2,'ep'=4,'tp'=4] {'ep'}, dimensions={0} | all-to-all | bytes 1572864 | tf_op jit(solution)/shard_map/all_to_all | solution.py:50
  46.4 0.0 all-gather.2.cloned.1.call-update
  46.5 0.0 reduce-scatter.3.cloned.1.call-start
  46.5 27.7 %all-gather.2.cloned.1.call-done = bf16[4,192,2048]{2,1,0:T(8,128)(2,1)} async-done(((bf16[4,192,512]{2,1,0:T(8,128)(2,1)}), bf16[4,192,2048]{2,1,0:T(8,128)(2,1)}) %all-gather.2.cloned.1.call-update) | async-done | bytes 3145744 | tf_op jit(solution)/shard_map/all_gather | solution.py:51
  74.2 0.0 copy-done.4
  74.2 3.8 %fusion.9 = f32[768,256]{1,0:T(8,128)} fusion(bf16[768,2048]{1,0:T(8,128)(2,1)} %bitcast.30, bf16[1,2048,256]{2,1,0:T(8,128)(2,1)S(1)} %copy-done.4), kind=kOutput, calls=%fused_computation.18 | convolution fusion | flops 805306368 | bytes 4980736 | tf_op jit(solution)/shard_map/dot_general | solution.py:58
  78.0 0.0 copy-done
  78.0 7.4 %convolution_convert_fusion = bf16[768,2048]{1,0:T(8,128)(2,1)} fusion(bf16[768,2048]{1,0:T(8,128)(2,1)} %bitcast.31, bf16[1,256,2048]{2,1,0:T(8,128)(2,1)S(1)} %copy-done, bf16[1,2048,256]{2,1,0:T(8,128)(2,1)} %param.15, f32[768,256]{1,0:T(8,128)} %fusion.9), kind=kOutput, calls=%fused_computation.3 | convolution fusion | flops 1613365248 | bytes 9175040 | tf_op jit(solution)/shard_map/dot_general | solution.py:64
  85.4 0.0 copy-start.1
  85.4 0.0 copy-start.2
  85.4 0.0 reduce-scatter.3.cloned.1.call-update
  85.4 0.0 reduce-scatter.5.cloned.1.call-start
  85.5 1.5 fusion.31
  87.0 0.0 copy-done.1
  87.0 0.0 copy-done.2
  87.0 0.0 copy-start.3
  87.0 1.8 %convolution_convert_fusion.1 = bf16[256,2048]{1,0:T(8,128)(2,1)} fusion(bf16[128,2048]{1,0:T(8,128)(2,1)S(1)} %copy-done.1, bf16[256,2048]{1,0:T(8,128)(2,1)S(1)} %fusion.2, bf16[2048,128]{1,0:T(8,128)(2,1)S(1)} %copy-done.2, f32[256,128]{1,0:T(8,128)S(1)} %fusion.31), kind=kOutput, calls=%fused_computation.6 | convolution fusion | flops 269156352 | bytes 3276800 | tf_op jit(solution)/shard_map/dot_general | solution.py:70
  88.8 0.0 reduce-scatter.5.cloned.1.call-update
  88.8 34.5 %reduce-scatter.3.cloned.1.call-done = bf16[768,512]{1,0:T(8,128)(2,1)} async-done(((bf16[768,2048]{1,0:T(8,128)(2,1)}), bf16[768,512]{1,0:T(8,128)(2,1)}) %reduce-scatter.3.cloned.1.call-update) | async-done | bytes 786448 | tf_op jit(solution)/shard_map/reduce_scatter | solution.py:72
  123.3 4.6 %all-to-all-start.1 = ((bf16[4,192,512]{2,1,0:T(8,128)(2,1)}), bf16[4,192,512]{2,1,0:T(8,128)(2,1)S(1)}, u32[]{:S(2)}, u32[]{:S(2)}) async-start(bf16[4,192,512]{2,1,0:T(8,128)(2,1)} %bitcast.26), calls=%async_computation.2 | async-start | bytes 1572864 | tf_op jit(solution)/shard_map/all_to_all | solution.py:80
  127.9 0.0 copy-done.3
  127.9 0.1 copy.14
  128.0 19.8 %all-to-all-done.1 = bf16[4,192,512]{2,1,0:T(8,128)(2,1)S(1)} async-done(((bf16[4,192,512]{2,1,0:T(8,128)(2,1)}), bf16[4,192,512]{2,1,0:T(8,128)(2,1)S(1)}, u32[]{:S(2)}, u32[]{:S(2)}) %all-to-all-start.1) | async-done | bytes 786464 | tf_op jit(solution)/shard_map/all_to_all | solution.py:80
  147.8 2.0 %gather_fusion.1 = bf16[512,512]{1,0:T(8,128)(2,1)S(1)} fusion(bf16[768,512]{1,0:T(8,128)(2,1)S(1)} %bitcast.24, s32[1024]{0:T(1024)S(1)} %pad_clamp_fusion), kind=kCustom, calls=%fused_computation.1 | custom fusion | bytes 1050624 | tf_op jit(solution)/shard_map/gather | solution.py:81
  149.8 0.7 reshape.65
  150.5 1.3 multiply_reduce_fusion
  151.8 0.0 reduce-scatter.5.cloned.1.call-done
  151.8 1.7 %add_convert_fusion = bf16[256,512]{1,0:T(8,128)(2,1)} fusion(f32[256,512]{1,0:T(8,128)S(1)} %multiply_reduce_fusion, bf16[256,512]{1,0:T(8,128)(2,1)} %reduce-scatter.5.cloned.1.call-done), kind=kLoop, calls=%fused_computation.27 | loop fusion | flops 393216 | bytes 1048576 | tf_op jit(solution)/shard_map/convert_element_type | solution.py:84
  (7 shorter events, 0.0 us)
Async XLA Ops:
  6.5 71.5 %copy-start = (bf16[1,256,2048]{2,1,0:T(8,128)(2,1)S(1)}, bf16[1,256,2048]{2,1,0:T(8,128)(2,1)}, u32[]{:S(2)}) copy-start(bf16[1,256,2048]{2,1,0:T(8,128)(2,1)} %param.16) | copy-start | bytes 3145732
  6.5 67.7 %all-gather.2.cloned.1.call-start = ((), (), s32[]{:S(2)}) async-start(), calls=%async_computation.4 | async-start | bytes 3932160 | tf_op jit(solution)/shard_map/all_gather | solution.py:51
  18.8 55.4 %copy-start.4 = (bf16[1,2048,256]{2,1,0:T(8,128)(2,1)S(1)}, bf16[1,2048,256]{2,1,0:T(8,128)(2,1)}, u32[]{:S(2)}) copy-start(bf16[1,2048,256]{2,1,0:T(8,128)(2,1)} %param.14) | copy-start | bytes 3145732
  46.5 76.8 %reduce-scatter.3.cloned.1.call-start = ((), (), s32[]{:S(2)}) async-start(), calls=%async_computation.5 | async-start | bytes 3932160 | tf_op jit(solution)/shard_map/reduce_scatter | solution.py:72
  85.4 1.6 %copy-start.1 = (bf16[128,2048]{1,0:T(8,128)(2,1)S(1)}, bf16[128,2048]{1,0:T(8,128)(2,1)}, u32[]{:S(2)}) copy-start(bf16[128,2048]{1,0:T(8,128)(2,1)} %param.19) | copy-start | bytes 1572868
  85.4 1.6 %copy-start.2 = (bf16[2048,128]{1,0:T(8,128)(2,1)S(1)}, bf16[2048,128]{1,0:T(8,128)(2,1)}, u32[]{:S(2)}) copy-start(bf16[2048,128]{1,0:T(8,128)(2,1)} %param.18) | copy-start | bytes 1572868
  85.4 66.4 %reduce-scatter.5.cloned.1.call-start = ((), (), s32[]{:S(2)}) async-start(), calls=%async_computation.6 | async-start | bytes 1310720 | tf_op jit(solution)/shard_map/reduce_scatter | solution.py:75
  87.0 40.9 %copy-start.3 = (f32[256,2]{0,1:T(2,128)S(1)}, f32[256,2]{0,1:T(2,128)}, u32[]{:S(2)}) copy-start(f32[256,2]{0,1:T(2,128)} %param.13) | copy-start | bytes 6148
  123.3 24.5 %all-to-all-start.1 = ((bf16[4,192,512]{2,1,0:T(8,128)(2,1)}), bf16[4,192,512]{2,1,0:T(8,128)(2,1)S(1)}, u32[]{:S(2)}, u32[]{:S(2)}) async-start(bf16[4,192,512]{2,1,0:T(8,128)(2,1)} %bitcast.26), calls=%async_computation.2 | async-start | bytes 1572864 | tf_op jit(solution)/shard_map/all_to_all | solution.py:80
Sparse Core Ops, SparseCore 0:
  46.6 27.6 all-gather.1
  85.5 37.7 reduce-scatter.2
  125.8 24.7 reduce-scatter.4
where the time goes:
time: 160 us
  waiting for transfers between devices  82 us (51%)
  blocking collectives  26.4 us (16%)
  matrix products  14.7 us (9%)
  between operations  13.3 us (8%)
  local copies, waits for them, and re-layouts  12.1 us (8%)
  other arithmetic  6.9 us (4%)
  starting transfers between devices  4.68 us (3%)
    reduce_scatter x1, waiting for transfers between devices, body(): lax.psum_scatter(routed_terms.astype(jnp.bfloat16), 'tp', scatter_dimensi...  34.5 us
    all_gather x1, waiting for transfers between devices, body(): piece = lax.all_gather(arrived, 'tp', axis=2, tiled=True)  27.7 us
    all_to_all x1, blocking collectives, body(): lax.all_to_all(own_columns, 'ep', split_axis=0, concat_axis=0, tiled=True)  26.4 us
    all_to_all x1, waiting for transfers between devices, body(): lax.all_to_all(expert_out, 'ep', split_axis=0, concat_axis=0, tiled=True)  19.8 us
    dot_general x1, matrix products, body(): jnp.dot(hidden, expert_down[local], preferred_element_type=jnp.float32)  7.39 us
    all_to_all x1, starting transfers between devices, body(): lax.all_to_all(expert_out, 'ep', split_axis=0, concat_axis=0, tiled=True)  4.6 us
    gather x1, local copies, waits for them, and re-layouts, body(): outgoing = padded[slot_token].reshape(experts, capacity, width)  4.27 us
    dot_general x1, matrix products, body(): gate_list = [jnp.dot(rows, gate_rows, preferred_element_type=jnp.float32)]  3.76 us
  transfers between devices with their start and end apart: 4, of which 3 were waited for; matrix products, arithmetic and copies ran while one was open for 5% of the time, Pallas kernels for 0%

commit v1 on v0

--- a/solution.py
+++ b/solution.py
@@ -1,6 +1,8 @@
 import jax
 import jax.numpy as jnp
 from jax import lax
+from jax.experimental import pallas as pl
+from jax.experimental.pallas import tpu as pltpu
 from jax.sharding import PartitionSpec as P
 
 
@@ -84,6 +86,250 @@
     return (routed + shared_sum).astype(jnp.bfloat16)
 
 
+MESH = pl.DeviceIdType.MESH
+
+
+def silu(v):
+    return v / (1.0 + jnp.exp(-v))
+
+
+def dot32(a, b):
+    return jnp.dot(a, b, preferred_element_type=jnp.float32)
+
+
+def make_kernel(ep_count, capacity):
+    others = list(range(1, ep_count))
+
+    def kernel(
+        tok_ref, gain_ref, routing_ref, gw_ref, wg_hbm, wu_hbm, wd_hbm, sg_hbm, su_hbm, sd_hbm,
+        out_ref,
+        wg, wu, wd, sg, su, sd, nq, pt, zsend, xq, esend, erecv, keep, fsend, frecv, gsend, grecv,
+        wsem, zs, zr, cs, cr, xs, xr, ds, dr, es, er, fs, fr, gs, gr,
+    ):
+        e = lax.axis_index("ep")
+        t = lax.axis_index("tp")
+        x = t // 2
+        c = t % 2
+        core = {"tp": t ^ 1}
+        across = {"tp": t ^ 2}
+        rows, width = tok_ref.shape
+        quarter = width // 4
+
+        barrier = pltpu.get_barrier_semaphore()
+        for k in others:
+            pl.semaphore_signal(barrier, inc=1, device_id={"ep": e ^ k}, device_id_type=MESH)
+        pl.semaphore_signal(barrier, inc=1, device_id=core, device_id_type=MESH)
+        pl.semaphore_signal(barrier, inc=1, device_id=across, device_id_type=MESH)
+
+        loads = [
+            pltpu.make_async_copy(a, b, wsem.at[i])
+            for i, (a, b) in enumerate(
+                [(wg_hbm, wg), (wu_hbm, wu), (sg_hbm, sg), (su_hbm, su), (wd_hbm, wd), (sd_hbm, sd)]
+            )
+        ]
+        for load in loads:
+            load.start()
+
+        values = tok_ref[...].astype(jnp.float32)
+        scale = lax.rsqrt(jnp.mean(values * values, axis=-1, keepdims=True) + 1e-06)
+        normed = (values * scale * gain_ref[...]).astype(jnp.bfloat16)
+        for q in range(4):
+            nq[q] = normed[:, q * quarter:(q + 1) * quarter]
+
+        lane = lax.broadcasted_iota(jnp.int32, (rows, 128), 1)
+        named = lane ^ e
+        hit = jnp.where(routing_ref[:, 0:1] == named, 1.0, 0.0)
+        weight = jnp.where(routing_ref[:, 0:1] == named, gw_ref[:, 0:1], 0.0)
+        for j in range(1, routing_ref.shape[1]):
+            hit = hit + jnp.where(routing_ref[:, j:j + 1] == named, 1.0, 0.0)
+            weight = weight + jnp.where(routing_ref[:, j:j + 1] == named, gw_ref[:, j:j + 1], 0.0)
+        earlier = (
+            lax.broadcasted_iota(jnp.int32, (rows, rows), 0)
+            > lax.broadcasted_iota(jnp.int32, (rows, rows), 1)
+        )
+        earlier = jnp.where(earlier, 1.0, 0.0).astype(jnp.bfloat16)
+        rank = dot32(earlier, hit.astype(jnp.bfloat16))
+        rank = jnp.where(hit > 0.5, rank, -1.0)
+        place = lax.broadcasted_iota(jnp.int32, (rows, capacity), 1).astype(jnp.float32)
+
+        def remote(src, dst, send, recv, to):
+            return pltpu.make_async_remote_copy(
+                src_ref=src, dst_ref=dst, send_sem=send, recv_sem=recv,
+                device_id=to, device_id_type=MESH,
+            )
+
+        zcopy, ccopy, xcopy, dcopy, ecopy, fcopy, gcopy = {}, {}, {}, {}, {}, {}, {}
+        for k in others:
+            i = k - 1
+            chosen = jnp.where(rank[:, k:k + 1] == place, 1.0, 0.0).astype(jnp.bfloat16)
+            pt[i] = chosen
+            packed = lax.dot_general(
+                chosen, nq[t], (((0,), (0,)), ((), ())), preferred_element_type=jnp.float32
+            )
+            zsend[i] = packed.astype(jnp.bfloat16)
+            if k == others[0]:
+                pl.semaphore_wait(barrier, len(others) + 2)
+            zcopy[k] = remote(zsend.at[i], xq.at[i, t], zs.at[i], zr.at[i], {"ep": e ^ k})
+            zcopy[k].start()
+
+        def columns(q):
+            return pl.ds(pl.multiple_of(q * quarter, quarter), quarter)
+
+        def hidden_of(pieces, w_gate, w_up):
+            gate, up = 0.0, 0.0
+            for q in range(4):
+                gate = gate + dot32(pieces(q), w_gate[q * quarter:(q + 1) * quarter, :])
+                up = up + dot32(pieces(q), w_up[q * quarter:(q + 1) * quarter, :])
+            return (silu(gate) * up).astype(jnp.bfloat16)
+
+        def exchange(r, n, product):
+            for j in range(2):
+                esend[r, j, :n] = product(columns(2 * j + 1 - c)).astype(jnp.bfloat16)
+            ecopy[r] = remote(
+                esend.at[r, :, pl.ds(0, n)], erecv.at[r, :, pl.ds(0, n)], es.at[r], er.at[r], core
+            )
+            ecopy[r].start()
+            for j in range(2):
+                keep[r, j, :n] = product(columns(2 * j + c))
+
+        def arrive(k):
+            i = k - 1
+            zcopy[k].wait_recv()
+            mine = xq.at[i, t]
+            xcopy[k] = remote(mine, mine, xs.at[i], xr.at[i], across)
+            xcopy[k].start()
+            ccopy[k] = remote(mine, mine, cs.at[i], cr.at[i], core)
+            ccopy[k].start()
+
+        def relay(k):
+            i = k - 1
+            xcopy[k].wait_recv()
+            theirs = xq.at[i, t ^ 2]
+            dcopy[k] = remote(theirs, theirs, ds.at[i], dr.at[i], core)
+            dcopy[k].start()
+
+        def expert(k):
+            i = k - 1
+            ccopy[k].wait_recv()
+            dcopy[k].wait_recv()
+            hidden = hidden_of(lambda q: xq[i, q], wg, wu)
+            exchange(k, capacity, lambda cols: dot32(hidden, wd[:, cols]))
+
+        def pair(r, n):
+            ecopy[r].wait_recv()
+            fsend[r, :n] = (
+                keep[r, 1 - x, :n] + erecv[r, 1 - x, :n].astype(jnp.float32)
+            ).astype(jnp.bfloat16)
+            fcopy[r] = remote(
+                fsend.at[r, pl.ds(0, n)], frecv.at[r, pl.ds(0, n)], fs.at[r], fr.at[r], across
+            )
+            fcopy[r].start()
+
+        def whole(r, n):
+            fcopy[r].wait_recv()
+            return (
+                keep[r, x, :n]
+                + erecv[r, x, :n].astype(jnp.float32)
+                + frecv[r, :n].astype(jnp.float32)
+            )
+
+        def give_back(k):
+            i = k - 1
+            gsend[i] = whole(k, capacity).astype(jnp.bfloat16)
+            gcopy[k] = remote(gsend.at[i], grecv.at[i], gs.at[i], gr.at[i], {"ep": e ^ k})
+            gcopy[k].start()
+
+        for load in loads:
+            load.wait()
+        own_hidden = hidden_of(lambda q: nq[q], wg, wu)
+        shared_hidden = hidden_of(lambda q: nq[q], sg, su)
+        exchange(
+            0,
+            rows,
+            lambda cols: dot32(own_hidden, wd[:, cols]) * weight[:, 0:1]
+            + dot32(shared_hidden, sd[:, cols]),
+        )
+        plan(arrive, relay, expert, pair, give_back, others, rows, capacity)
+
+        total = whole(0, rows)
+        for k in others:
+            gcopy[k].wait_recv()
+            total = total + dot32(pt[k - 1], grecv[k - 1]) * weight[:, k:k + 1]
+        out_ref[...] = total.astype(out_ref.dtype)
+
+        for group in (zcopy, ccopy, xcopy, dcopy, ecopy, fcopy, gcopy):
+            for copy in group.values():
+                copy.wait_send()
+
+    return kernel
+
+
+def plan(arrive, relay, expert, pair, give_back, others, rows, capacity):
+    previous = None
+    for k in others:
+        arrive(k)
+        if previous is None:
+            pair(0, rows)
+        else:
+            give_back(previous)
+        relay(k)
+        expert(k)
+        pair(k, capacity)
+        previous = k
+    give_back(previous)
+
+
+def fused_body(
+    tokens, norm_gain, routing, gate_weights,
+    expert_gate, expert_up, expert_down, shared_gate, shared_up, shared_down,
+):
+    n = lax.axis_size("ep")
+    rows, width = tokens.shape
+    capacity = max(2, 3 * rows * routing.shape[1] // (2 * n))
+    quarter = width // 4
+    ffe = expert_gate.shape[2]
+    ffs = shared_gate.shape[1]
+    o = n - 1
+    bf16, f32 = jnp.bfloat16, jnp.float32
+    big = max(rows, capacity)
+    dma = pltpu.SemaphoreType.DMA
+    vmem = pl.BlockSpec(memory_space=pltpu.VMEM)
+    hbm = pl.BlockSpec(memory_space=pl.ANY)
+    return pl.pallas_call(
+        make_kernel(n, capacity),
+        out_shape=jax.ShapeDtypeStruct((rows, quarter), bf16),
+        in_specs=[vmem] * 4 + [hbm] * 6,
+        out_specs=vmem,
+        scratch_shapes=[
+            pltpu.VMEM((width, ffe), bf16),
+            pltpu.VMEM((width, ffe), bf16),
+            pltpu.VMEM((ffe, width), bf16),
+            pltpu.VMEM((width, ffs), bf16),
+            pltpu.VMEM((width, ffs), bf16),
+            pltpu.VMEM((ffs, width), bf16),
+            pltpu.VMEM((4, rows, quarter), bf16),
+            pltpu.VMEM((o, rows, capacity), bf16),
+            pltpu.VMEM((o, capacity, quarter), bf16),
+            pltpu.VMEM((o, 4, capacity, quarter), bf16),
+            pltpu.VMEM((n, 2, big, quarter), bf16),
+            pltpu.VMEM((n, 2, big, quarter), bf16),
+            pltpu.VMEM((n, 2, big, quarter), f32),
+            pltpu.VMEM((n, big, quarter), bf16),
+            pltpu.VMEM((n, big, quarter), bf16),
+            pltpu.VMEM((o, capacity, quarter), bf16),
+            pltpu.VMEM((o, capacity, quarter), bf16),
+            dma((6,)),
+        ]
+        + [dma((o,))] * 8
+        + [dma((n,))] * 4
+        + [dma((o,))] * 2,
+        compiler_params=pltpu.CompilerParams(collective_id=0, has_side_effects=True),
+    )(
+        tokens, norm_gain.reshape(1, width), routing, gate_weights,
+        expert_gate[0], expert_up[0], expert_down[0], shared_gate, shared_up, shared_down,
+    )
+
+
 def solution(mesh):
     in_specs = (
         P(("grp", "ep"), None),
@@ -98,4 +344,13 @@
         P("tp", None),
     )
     out_specs = P(("grp", "ep"), "tp")
-    return jax.shard_map(body, mesh=mesh, in_specs=in_specs, out_specs=out_specs, check_vma=False)
+    ep_count, tp_count = mesh.shape["ep"], mesh.shape["tp"]
+
+    def layer(*args):
+        few = tp_count == 4 and ep_count in (2, 4) and args[4].shape[0] == ep_count
+        chosen = fused_body if few else body
+        return jax.shard_map(
+            chosen, mesh=mesh, in_specs=in_specs, out_specs=out_specs, check_vma=False
+        )(*args)
+
+    return layer

time: 160 us -> 67.3 us (0.42)
  waiting for transfers between devices: 82 us -> 0 us
  Pallas kernels: 0 us -> 63.2 us
  blocking collectives: 26.4 us -> 0 us
  matrix products: 14.7 us -> 0 us
  between operations: 13.3 us -> 0.01 us
  local copies, waits for them, and re-layouts: 12.1 us -> 3.95 us
  other arithmetic: 6.9 us -> 0 us
  starting transfers between devices: 4.68 us -> 0 us
    pallas_call x0 -> x1, Pallas kernels: none -> 63.2 us  [fused_body(): pl.pallas_call(make_kernel(n, capacity), out_shape=jax.ShapeDtypeStruct((...]
    reduce_scatter x2 -> x0, waiting for transfers between devices: 34.5 us -> none  [the longest x1 34.5 us: body(): lax.psum_scatter(routed_terms.astype(jnp.bfloat16), 'tp', scatter_dimensi...]
    all_gather x1 -> x0, waiting for transfers between devices: 27.7 us -> none  [body(): piece = lax.all_gather(arrived, 'tp', axis=2, tiled=True)]
    all_to_all x1 -> x0, blocking collectives: 26.4 us -> none  [body(): lax.all_to_all(own_columns, 'ep', split_axis=0, concat_axis=0, tiled=True)]
    all_to_all x1 -> x0, waiting for transfers between devices: 19.8 us -> none  [body(): lax.all_to_all(expert_out, 'ep', split_axis=0, concat_axis=0, tiled=True)]
    dot_general x5 -> x0, matrix products: 14.7 us -> none  [the longest x1 7.39 us: body(): jnp.dot(hidden, expert_down[local], preferred_element_type=jnp.float32)]
    gather x2 -> x0, local copies, waits for them, and re-layouts: 6.23 us -> none  [the longest x1 4.27 us: body(): outgoing = padded[slot_token].reshape(experts, capacity, width)]
    all_to_all x1 -> x0, starting transfers between devices: 4.6 us -> none  [body(): lax.all_to_all(expert_out, 'ep', split_axis=0, concat_axis=0, tiled=True)]
  transfers between devices with their start and end apart: 4 -> 0, of which waited for: 3 -> 0; matrix products, arithmetic and copies ran while one was open for 5% -> 0% of each run, Pallas kernels for 0% -> 0%
where the time goes in v1:
time: 67.3 us; the launch traced here: 67.1 us
  Pallas kernels  63.2 us (94%)
  local copies, waits for them, and re-layouts  3.95 us (6%)
    pallas_call x1, Pallas kernels, fused_body(): pl.pallas_call(make_kernel(n, capacity), out_shape=jax.ShapeDtypeStruct((...  63.2 us
    unnamed x7, local copies, waits for them, and re-layouts  3.95 us

profile of v1, /device:TPU:0, one launch (start us, length us, event | category | flops | bytes accessed | tf_op | source)
XLA Modules:
  0.0 67.1 jit_solution(3687318297234643312)
XLA Ops:
  0.0 0.0 copy-start
  0.0 0.7 %copy-done = s32[256,2]{0,1:T(2,128)S(1)} copy-done((s32[256,2]{0,1:T(2,128)S(1)}, s32[256,2]{0,1:T(2,128)}, u32[]{:S(2)}) %copy-start) | copy-done | bytes 2072
  0.7 0.0 copy-start.1
  0.7 0.8 %copy.11.routing_ref = s32[256,2]{1,0:T(8,128)} copy(s32[256,2]{0,1:T(2,128)S(1)} %copy-done) | data formatting | bytes 4096 | tf_op args[2]
  1.5 0.0 copy-done.1
  1.5 0.8 %copy.12.gw_ref = f32[256,2]{1,0:T(8,128)} copy(f32[256,2]{0,1:T(2,128)S(1)} %copy-done.1) | data formatting | bytes 4096 | tf_op args[3]
  2.3 63.2 %shard_map.100 = bf16[256,512]{1,0:T(8,128)(2,1)} custom-call(bf16[256,2048]{1,0:T(8,128)(2,1)} %tok_ref.1, f32[1,2048]{1,0:T(1,128)} %bitcast.7, s32[256,2]{1,0:T(8,128)} %copy.11.routing_ref, f32[256,2]{1,0:T(8,128)} %copy.12.gw_ref, bf16[2048,256]{1,0:T(8,128)(2,1)} %bitcast.4, bf16[2048,256]{1,0:T(8,128)(2,1)} %bitcast.5, bf16[256,2048]{1,0:T(8,128)(2,1)} %bitcast.6, ...), custom_call_target="tpu_custom_call" | custom-call | tf_op jit(solution)/shard_map/pallas_call | solution.py:298
  65.5 1.7 %copy.14 = bf16[256,512]{1,0:T(8,128)(2,1)} copy(bf16[256,512]{1,0:T(8,128)(2,1)} %shard_map.100) | data formatting | bytes 524288
Async XLA Ops:
  0.0 0.7 %copy-start = (s32[256,2]{0,1:T(2,128)S(1)}, s32[256,2]{0,1:T(2,128)}, u32[]{:S(2)}) copy-start(s32[256,2]{0,1:T(2,128)} %param.12) | copy-start | bytes 6148
  0.7 0.8 %copy-start.1 = (f32[256,2]{0,1:T(2,128)S(1)}, f32[256,2]{0,1:T(2,128)}, u32[]{:S(2)}) copy-start(f32[256,2]{0,1:T(2,128)} %param.13) | copy-start | bytes 6148

commit v2 on v1

--- a/solution.py
+++ b/solution.py
@@ -97,8 +97,10 @@
     return jnp.dot(a, b, preferred_element_type=jnp.float32)
 
 
-def make_kernel(ep_count, capacity):
+def make_kernel(ep_count, capacity, halves):
     others = list(range(1, ep_count))
+    part = capacity // halves
+    items = list(range(len(others) * halves))
 
     def kernel(
         tok_ref, gain_ref, routing_ref, gw_ref, wg_hbm, wu_hbm, wd_hbm, sg_hbm, su_hbm, sd_hbm,
@@ -115,6 +117,9 @@
         rows, width = tok_ref.shape
         quarter = width // 4
 
+        def partner(i):
+            return {"ep": e ^ (i // halves + 1)}
+
         barrier = pltpu.get_barrier_semaphore()
         for k in others:
             pl.semaphore_signal(barrier, inc=1, device_id={"ep": e ^ k}, device_id_type=MESH)
@@ -136,21 +141,22 @@
         for q in range(4):
             nq[q] = normed[:, q * quarter:(q + 1) * quarter]
 
-        lane = lax.broadcasted_iota(jnp.int32, (rows, 128), 1)
-        named = lane ^ e
-        hit = jnp.where(routing_ref[:, 0:1] == named, 1.0, 0.0)
-        weight = jnp.where(routing_ref[:, 0:1] == named, gw_ref[:, 0:1], 0.0)
-        for j in range(1, routing_ref.shape[1]):
-            hit = hit + jnp.where(routing_ref[:, j:j + 1] == named, 1.0, 0.0)
-            weight = weight + jnp.where(routing_ref[:, j:j + 1] == named, gw_ref[:, j:j + 1], 0.0)
+        named = lax.broadcasted_iota(jnp.int32, (16, rows), 0) ^ e
+        hit = jnp.zeros((16, rows), jnp.float32)
+        weight = jnp.zeros((16, rows), jnp.float32)
+        for j in range(routing_ref.shape[0]):
+            same = routing_ref[j:j + 1, :] == named
+            hit = hit + jnp.where(same, 1.0, 0.0)
+            weight = weight + jnp.where(same, gw_ref[j:j + 1, :], 0.0)
+        weight = weight.T
         earlier = (
             lax.broadcasted_iota(jnp.int32, (rows, rows), 0)
-            > lax.broadcasted_iota(jnp.int32, (rows, rows), 1)
+            < lax.broadcasted_iota(jnp.int32, (rows, rows), 1)
         )
         earlier = jnp.where(earlier, 1.0, 0.0).astype(jnp.bfloat16)
-        rank = dot32(earlier, hit.astype(jnp.bfloat16))
+        rank = dot32(hit.astype(jnp.bfloat16), earlier)
         rank = jnp.where(hit > 0.5, rank, -1.0)
-        place = lax.broadcasted_iota(jnp.int32, (rows, capacity), 1).astype(jnp.float32)
+        place = lax.broadcasted_iota(jnp.int32, (part, rows), 0)
 
         def remote(src, dst, send, recv, to):
             return pltpu.make_async_remote_copy(
@@ -159,18 +165,16 @@
             )
 
         zcopy, ccopy, xcopy, dcopy, ecopy, fcopy, gcopy = {}, {}, {}, {}, {}, {}, {}
-        for k in others:
-            i = k - 1
-            chosen = jnp.where(rank[:, k:k + 1] == place, 1.0, 0.0).astype(jnp.bfloat16)
+        for i in items:
+            k, h = i // halves + 1, i % halves
+            wanted = (place + h * part).astype(jnp.float32)
+            chosen = jnp.where(rank[k:k + 1, :] == wanted, 1.0, 0.0).astype(jnp.bfloat16)
             pt[i] = chosen
-            packed = lax.dot_general(
-                chosen, nq[t], (((0,), (0,)), ((), ())), preferred_element_type=jnp.float32
-            )
-            zsend[i] = packed.astype(jnp.bfloat16)
-            if k == others[0]:
+            zsend[i] = dot32(chosen, nq[t]).astype(jnp.bfloat16)
+            if i == 0:
                 pl.semaphore_wait(barrier, len(others) + 2)
-            zcopy[k] = remote(zsend.at[i], xq.at[i, t], zs.at[i], zr.at[i], {"ep": e ^ k})
-            zcopy[k].start()
+            zcopy[i] = remote(zsend.at[i], xq.at[i, t], zs.at[i], zr.at[i], partner(i))
+            zcopy[i].start()
 
         def columns(q):
             return pl.ds(pl.multiple_of(q * quarter, quarter), quarter)
@@ -192,28 +196,25 @@
             for j in range(2):
                 keep[r, j, :n] = product(columns(2 * j + c))
 
-        def arrive(k):
-            i = k - 1
-            zcopy[k].wait_recv()
+        def arrive(i):
+            zcopy[i].wait_recv()
             mine = xq.at[i, t]
-            xcopy[k] = remote(mine, mine, xs.at[i], xr.at[i], across)
-            xcopy[k].start()
-            ccopy[k] = remote(mine, mine, cs.at[i], cr.at[i], core)
-            ccopy[k].start()
-
-        def relay(k):
-            i = k - 1
-            xcopy[k].wait_recv()
+            xcopy[i] = remote(mine, mine, xs.at[i], xr.at[i], across)
+            xcopy[i].start()
+            ccopy[i] = remote(mine, mine, cs.at[i], cr.at[i], core)
+            ccopy[i].start()
+
+        def relay(i):
+            xcopy[i].wait_recv()
             theirs = xq.at[i, t ^ 2]
-            dcopy[k] = remote(theirs, theirs, ds.at[i], dr.at[i], core)
-            dcopy[k].start()
-
-        def expert(k):
-            i = k - 1
-            ccopy[k].wait_recv()
-            dcopy[k].wait_recv()
+            dcopy[i] = remote(theirs, theirs, ds.at[i], dr.at[i], core)
+            dcopy[i].start()
+
+        def expert(i):
+            ccopy[i].wait_recv()
+            dcopy[i].wait_recv()
             hidden = hidden_of(lambda q: xq[i, q], wg, wu)
-            exchange(k, capacity, lambda cols: dot32(hidden, wd[:, cols]))
+            exchange(1 + i, part, lambda cols: dot32(hidden, wd[:, cols]))
 
         def pair(r, n):
             ecopy[r].wait_recv()
@@ -233,11 +234,10 @@
                 + frecv[r, :n].astype(jnp.float32)
             )
 
-        def give_back(k):
-            i = k - 1
-            gsend[i] = whole(k, capacity).astype(jnp.bfloat16)
-            gcopy[k] = remote(gsend.at[i], grecv.at[i], gs.at[i], gr.at[i], {"ep": e ^ k})
-            gcopy[k].start()
+        def give_back(i):
+            gsend[i] = whole(1 + i, part).astype(jnp.bfloat16)
+            gcopy[i] = remote(gsend.at[i], grecv.at[i], gs.at[i], gr.at[i], partner(i))
+            gcopy[i].start()
 
         for load in loads:
             load.wait()
@@ -249,12 +249,16 @@
             lambda cols: dot32(own_hidden, wd[:, cols]) * weight[:, 0:1]
             + dot32(shared_hidden, sd[:, cols]),
         )
-        plan(arrive, relay, expert, pair, give_back, others, rows, capacity)
+        plan(arrive, relay, expert, pair, give_back, len(items), rows, part)
 
         total = whole(0, rows)
-        for k in others:
-            gcopy[k].wait_recv()
-            total = total + dot32(pt[k - 1], grecv[k - 1]) * weight[:, k:k + 1]
+        for i in items:
+            k = i // halves + 1
+            gcopy[i].wait_recv()
+            placed = lax.dot_general(
+                pt[i], grecv[i], (((0,), (0,)), ((), ())), preferred_element_type=jnp.float32
+            )
+            total = total + placed * weight[:, k:k + 1]
         out_ref[...] = total.astype(out_ref.dtype)
 
         for group in (zcopy, ccopy, xcopy, dcopy, ecopy, fcopy, gcopy):
@@ -264,19 +268,20 @@
     return kernel
 
 
-def plan(arrive, relay, expert, pair, give_back, others, rows, capacity):
-    previous = None
-    for k in others:
-        arrive(k)
-        if previous is None:
+def plan(arrive, relay, expert, pair, give_back, count, rows, part):
+    for step in range(count + 3):
+        if step < count:
+            arrive(step)
+        if step == 0:
             pair(0, rows)
-        else:
-            give_back(previous)
-        relay(k)
-        expert(k)
-        pair(k, capacity)
-        previous = k
-    give_back(previous)
+        if 0 <= step - 3 < count:
+            give_back(step - 3)
+        if 0 <= step - 1 < count:
+            relay(step - 1)
+        if 0 <= step - 2 < count:
+            pair(1 + step - 2, part)
+        if 0 <= step - 1 < count:
+            expert(step - 1)
 
 
 def fused_body(
@@ -289,14 +294,16 @@
     quarter = width // 4
     ffe = expert_gate.shape[2]
     ffs = shared_gate.shape[1]
-    o = n - 1
+    halves = 2 if capacity % 32 == 0 else 1
+    part = capacity // halves
+    o = (n - 1) * halves
     bf16, f32 = jnp.bfloat16, jnp.float32
-    big = max(rows, capacity)
+    big = max(rows, part)
     dma = pltpu.SemaphoreType.DMA
     vmem = pl.BlockSpec(memory_space=pltpu.VMEM)
     hbm = pl.BlockSpec(memory_space=pl.ANY)
     return pl.pallas_call(
-        make_kernel(n, capacity),
+        make_kernel(n, capacity, halves),
         out_shape=jax.ShapeDtypeStruct((rows, quarter), bf16),
         in_specs=[vmem] * 4 + [hbm] * 6,
         out_specs=vmem,
@@ -308,24 +315,24 @@
             pltpu.VMEM((width, ffs), bf16),
             pltpu.VMEM((ffs, width), bf16),
             pltpu.VMEM((4, rows, quarter), bf16),
-            pltpu.VMEM((o, rows, capacity), bf16),
-            pltpu.VMEM((o, capacity, quarter), bf16),
-            pltpu.VMEM((o, 4, capacity, quarter), bf16),
-            pltpu.VMEM((n, 2, big, quarter), bf16),
-            pltpu.VMEM((n, 2, big, quarter), bf16),
-            pltpu.VMEM((n, 2, big, quarter), f32),
-            pltpu.VMEM((n, big, quarter), bf16),
-            pltpu.VMEM((n, big, quarter), bf16),
-            pltpu.VMEM((o, capacity, quarter), bf16),
-            pltpu.VMEM((o, capacity, quarter), bf16),
+            pltpu.VMEM((o, part, rows), bf16),
+            pltpu.VMEM((o, part, quarter), bf16),
+            pltpu.VMEM((o, 4, part, quarter), bf16),
+            pltpu.VMEM((o + 1, 2, big, quarter), bf16),
+            pltpu.VMEM((o + 1, 2, big, quarter), bf16),
+            pltpu.VMEM((o + 1, 2, big, quarter), f32),
+            pltpu.VMEM((o + 1, big, quarter), bf16),
+            pltpu.VMEM((o + 1, big, quarter), bf16),
+            pltpu.VMEM((o, part, quarter), bf16),
+            pltpu.VMEM((o, part, quarter), bf16),
             dma((6,)),
         ]
         + [dma((o,))] * 8
-        + [dma((n,))] * 4
+        + [dma((o + 1,))] * 4
         + [dma((o,))] * 2,
         compiler_params=pltpu.CompilerParams(collective_id=0, has_side_effects=True),
     )(
-        tokens, norm_gain.reshape(1, width), routing, gate_weights,
+        tokens, norm_gain.reshape(1, width), routing.T, gate_weights.T,
         expert_gate[0], expert_up[0], expert_down[0], shared_gate, shared_up, shared_down,
     )
 

time: 67.3 us -> 56.8 us (0.84)
  the two profiles are of different devices: /device:TPU:0 before, /device:TPU:17 now
where the time goes in v2:
time: 56.8 us; the launch traced here: 56.7 us
  Pallas kernels  55 us (97%)
  local copies, waits for them, and re-layouts  1.67 us (3%)
    pallas_call x1, Pallas kernels, fused_body(): pl.pallas_call(make_kernel(n, capacity, halves), out_shape=jax.ShapeDtype...  55 us
    unnamed x1, local copies, waits for them, and re-layouts  1.67 us

profile of v2, /device:TPU:17, one launch (start us, length us, event | category | flops | bytes accessed | tf_op | source)
XLA Modules:
  0.0 56.7 jit_solution(15794173413324358805)
XLA Ops:
  0.0 55.0 %shard_map.100 = bf16[256,512]{1,0:T(8,128)(2,1)} custom-call(bf16[256,2048]{1,0:T(8,128)(2,1)} %tok_ref.1, f32[1,2048]{1,0:T(1,128)} %bitcast.9, s32[2,256]{1,0:T(2,128)} %bitcast.10, f32[2,256]{1,0:T(2,128)} %bitcast.11, bf16[2048,256]{1,0:T(8,128)(2,1)} %bitcast.6, bf16[2048,256]{1,0:T(8,128)(2,1)} %bitcast.7, bf16[256,2048]{1,0:T(8,128)(2,1)} %bitcast.8, ...), custom_call_target="tpu_custom_call" | custom-call | tf_op jit(solution)/shard_map/pallas_call | solution.py:305
  55.0 1.7 %copy.12 = bf16[256,512]{1,0:T(8,128)(2,1)} copy(bf16[256,512]{1,0:T(8,128)(2,1)} %shard_map.100) | data formatting | bytes 524288
